TPU v7x, 256 devices: a 4x2x16 block of a 4x16x16 slice. The times are simulated.
256 devices in a mesh: grp: 2 (over y), st: 32 (over z, core), tp: 4 (over x).
Axes of the slice: x: 4, y: 2, z: 16, core: 2. Of those that a mesh axis runs over, the one named last changes fastest.
The devices are a block of a 4x16x16 slice.
Arguments:
- pass_ids: int32 [512, 4], P(('grp', 'st')), parts along dimension 0, may hold values from 0 to 511, as said below
- store: bfloat16 [512, 64, 2048], P('st', None, 'tp'), may hold values from -6 to 6
- queries: bfloat16 [65536, 1024], P(('grp', 'st'), 'tp'), parts along dimension 0, may hold values from -40 to 40
- gate_pre: bfloat16 [65536, 1024], P(('grp', 'st'), 'tp'), parts along dimension 0, may hold values from -6 to 6
- w_query: bfloat16 [2048, 1024], P(None, 'tp'), may hold values from -0.125 to 0.125
- w_gate: bfloat16 [2048, 1024], P(None, 'tp'), may hold values from -0.125 to 0.125
- w_key: bfloat16 [2048, 1024], P(None, 'tp'), may hold values from -0.125 to 0.125
- w_value: bfloat16 [2048, 1024], P(None, 'tp'), may hold values from -0.125 to 0.125
- d_mem: bfloat16 [65536, 1024], P(('grp', 'st'), 'tp'), parts along dimension 0, may hold values from -6 to 6
Outputs:
- d_tokens: bfloat16 [65536, 2048], P(('grp', 'st', 'tp')), parts along dimension 0
- d_store: bfloat16 [1024, 64, 2048], P(('grp', 'st', 'tp')), parts along dimension 0
- d_wkey: float32 [4096, 1024], P(('grp', 'st'), 'tp'), parts along dimension 0
There are 2 independent parts, one for each index of `grp`. A program takes and returns all parts, laid end to end along the dimension named above; an argument that names none is the same for every part. Nothing has to cross between parts.
Inputs may be any that keep to these rules, and one draw needn't show every extreme that they name: `pass_ids`: the 8 blocks of one index of st name at most 2 passages (counted with repetition) held by any one index of st o, that is passages o * 16 to o * 16 + 15. Every index of st takes exactly 2 passages from each of 16 indices of st and none from the others, so the bound 2 is reached by every index.
All inputs are finite; a program needn't handle non-finite values.
Results may differ from a plain program's by a relative error of at most 0.02.
Values may be sent and summed in bfloat16 or wider, within the bound.
A program may use at most 128 MiB of HBM per device.

v0:
```python
import jax
import jax.numpy as jnp
from jax import lax
from jax.sharding import Mesh
from jax.sharding import PartitionSpec as P

HD = 256
BLK = 128
PB = 4
ST = ("st_0", "st_1")
GRP_ST = ("grp", "st_0", "st_1")
GRP_ST_TP = ("grp", "st_0", "st_1", "tp")


def sum_in_order(tiles, axes, order):
    dims = [lax.axis_size(a) for a in axes]
    tiles = tiles.reshape(*dims, *tiles.shape[1:])
    tiles = tiles.transpose(*order, *range(len(axes), tiles.ndim))
    tiles = tiles.reshape(-1, *tiles.shape[len(axes) :])
    for k in order:
        tiles = lax.psum_scatter(tiles, axes[k], scatter_dimension=0, tiled=True)
    return tiles[0]


def in_blocks(array, dim, devices):
    before, after = (array.shape[:dim], array.shape[dim + 1 :])
    return jnp.moveaxis(array.reshape(*before, devices, -1, *after), dim, 0)


def summed_rows_2(array, axes, order, dim):
    devices = lax.axis_size(axes)
    return sum_in_order(in_blocks(array, dim, devices), axes, order)


def summed_on_arrival(array, axis, dim):
    devices = lax.axis_size(axis)
    tiles = lax.all_to_all(in_blocks(array, dim, devices), axis, 0, 0, tiled=True)
    return jnp.sum(tiles.astype(jnp.float32), axis=0)


def local(pass_ids, store, queries, gate_pre, w_query, w_gate, w_key, w_value, d_mem):
    st_count = lax.axis_size(ST)
    tp_count = lax.axis_size("tp")
    tok_rows, head_cols = queries.shape
    head_count = head_cols // HD
    blocks = tok_rows // BLK
    passages = store.shape[0]
    pass_len = store.shape[1]
    model_width = w_key.shape[0]
    requests = blocks * PB
    slot_depth = max(2, requests // st_count)
    slot_total = st_count * slot_depth
    pair_cols = 2 * head_cols
    request_ids = pass_ids.reshape(-1)
    owners = request_ids // passages
    within = request_ids % passages
    owner_hot = (owners[:, None] == jnp.arange(st_count, dtype=jnp.int32)[None, :]).astype(
        jnp.int32
    )
    ranking = jnp.sum(jnp.cumsum(owner_hot, axis=0) * owner_hot, axis=1) - 1
    slot_index = owners * slot_depth + ranking
    slot_hot = slot_index[:, None] == jnp.arange(slot_total, dtype=jnp.int32)[None, :]
    wanted = jnp.max(jnp.where(slot_hot, within[:, None], -1), axis=0).reshape(st_count, slot_depth)
    asked_rows = lax.all_to_all(wanted, ST, split_axis=0, concat_axis=0, tiled=True).reshape(-1)
    weight_kv = jnp.concatenate([w_key, w_value], axis=1)
    gathered = lax.all_gather(store, "tp", axis=2, tiled=True)
    flat_rows = gathered.reshape(passages * pass_len, model_width)
    kv_pass = jnp.dot(flat_rows, weight_kv, preferred_element_type=jnp.float32)
    kv_low = kv_pass.astype(jnp.bfloat16).reshape(passages, pass_len * pair_cols)
    pick_rows = (asked_rows[:, None] == jnp.arange(passages, dtype=jnp.int32)[None, :]).astype(
        jnp.bfloat16
    )
    outgoing = jnp.dot(pick_rows, kv_low, preferred_element_type=jnp.float32).astype(jnp.bfloat16)
    incoming = lax.all_to_all(
        outgoing.reshape(st_count, slot_depth, pass_len, pair_cols),
        ST,
        split_axis=0,
        concat_axis=0,
        tiled=True,
    )
    request_kv = incoming.reshape(slot_total, pass_len, pair_cols)[slot_index]
    block_kv = request_kv.reshape(blocks, PB * pass_len, pair_cols)
    key_rows = block_kv[:, :, :head_cols].reshape(blocks, PB * pass_len, head_count, HD)
    value_rows = block_kv[:, :, head_cols:].reshape(blocks, PB * pass_len, head_count, HD)
    query_rows = queries.reshape(blocks, BLK, head_count, HD)
    score_scale = HD ** (-0.5)
    scores = (
        jnp.einsum("nqhd,nkhd->nhqk", query_rows, key_rows, preferred_element_type=jnp.float32)
        * score_scale
    )
    shifted = jnp.exp(scores - jnp.max(scores, axis=-1, keepdims=True))
    prob_rows = shifted / jnp.sum(shifted, axis=-1, keepdims=True)
    probs_low = prob_rows.astype(jnp.bfloat16)
    attended = jnp.einsum(
        "nhqk,nkhd->nqhd", probs_low, value_rows, preferred_element_type=jnp.float32
    ).reshape(tok_rows, head_cols)
    gate_vals = gate_pre.astype(jnp.float32)
    sigmoid_vals = jax.nn.sigmoid(gate_vals)
    mem_grad = d_mem.astype(jnp.float32)
    attended_grad = (gate_vals * sigmoid_vals * mem_grad).astype(jnp.bfloat16)
    gate_grad = (
        mem_grad * attended * sigmoid_vals * (1.0 + gate_vals * (1.0 - sigmoid_vals))
    ).astype(jnp.bfloat16)
    attended_four = attended_grad.reshape(blocks, BLK, head_count, HD)
    prob_grad = jnp.einsum(
        "nqhd,nkhd->nhqk", attended_four, value_rows, preferred_element_type=jnp.float32
    )
    score_grad = (
        score_scale
        * prob_rows
        * (prob_grad - jnp.sum(prob_rows * prob_grad, axis=-1, keepdims=True))
    ).astype(jnp.bfloat16)
    query_grad = (
        jnp.einsum("nhqk,nkhd->nqhd", score_grad, key_rows, preferred_element_type=jnp.float32)
        .astype(jnp.bfloat16)
        .reshape(tok_rows, head_cols)
    )
    key_grad = jnp.einsum(
        "nhqk,nqhd->nkhd", score_grad, query_rows, preferred_element_type=jnp.float32
    )
    value_grad = jnp.einsum(
        "nhqk,nqhd->nkhd", probs_low, attended_four, preferred_element_type=jnp.float32
    )
    request_grads = jnp.concatenate(
        [
            key_grad.reshape(blocks, PB * pass_len, head_cols),
            value_grad.reshape(blocks, PB * pass_len, head_cols),
        ],
        axis=2,
    )
    request_grads = request_grads.astype(jnp.bfloat16).reshape(requests, pass_len * pair_cols)
    returning = jnp.dot(
        slot_hot.T.astype(jnp.bfloat16), request_grads, preferred_element_type=jnp.float32
    ).astype(jnp.bfloat16)
    arrived = lax.all_to_all(
        returning.reshape(st_count, slot_depth, pass_len, pair_cols),
        ST,
        split_axis=0,
        concat_axis=0,
        tiled=True,
    )
    pass_grad = jnp.dot(
        pick_rows.T,
        arrived.reshape(slot_total, pass_len * pair_cols),
        preferred_element_type=jnp.float32,
    )
    pass_low = pass_grad.astype(jnp.bfloat16).reshape(passages, pass_len, pair_cols)
    key_sums = pass_low[:, :, :head_cols].reshape(passages * pass_len, head_cols)
    d_wkey = summed_rows_2(
        jnp.einsum("rc,rh->ch", flat_rows, key_sums, preferred_element_type=jnp.float32),
        ST,
        (1, 0),
        0,
    )
    partial_value = pass_low.reshape(
        passages // tp_count * lax.axis_size("tp") * pass_len, pair_cols
    )
    d_store = summed_on_arrival(
        jnp.einsum("rc,dc->rd", partial_value, weight_kv, preferred_element_type=jnp.float32)
        .reshape(passages // tp_count * lax.axis_size("tp"), pass_len, model_width)
        .astype(jnp.bfloat16),
        "tp",
        0,
    ).astype(jnp.bfloat16)
    grad_both = jnp.concatenate([query_grad, gate_grad], axis=1)
    weight_both = jnp.concatenate([w_query, w_gate], axis=1)
    partial_value = grad_both
    d_tokens = summed_on_arrival(
        jnp.einsum(
            "rc,dc->rd", partial_value, weight_both, preferred_element_type=jnp.float32
        ).astype(jnp.bfloat16),
        "tp",
        0,
    ).astype(jnp.bfloat16)
    return (d_tokens, d_store, d_wkey)


def solution(mesh):
    finer = Mesh(
        mesh.devices.reshape(mesh.shape["grp"], 16, 2, mesh.shape["tp"]),
        ("grp", "st_0", "st_1", "tp"),
    )
    in_specs = (
        P(GRP_ST, None),
        P(ST, None, "tp"),
        P(GRP_ST, "tp"),
        P(GRP_ST, "tp"),
        P(None, "tp"),
        P(None, "tp"),
        P(None, "tp"),
        P(None, "tp"),
        P(GRP_ST, "tp"),
    )
    out_specs = (P(GRP_ST_TP, None), P(GRP_ST_TP, None, None), P(GRP_ST, "tp"))
    return jax.shard_map(local, mesh=finer, in_specs=in_specs, out_specs=out_specs, check_vma=False)
```

profile of v0, /device:TPU:34, one launch (start us, length us, event | category | flops | bytes accessed | tf_op | source)
XLA Modules:
  0.0 645.7 jit_solution(13220018644907863382)
XLA Ops:
  10.0 24.7 %all-to-all-start = ((s32[32,1,2]{2,1,0:T(1,128)}), s32[32,1,2]{2,1,0:T(1,128)S(1)}, u32[]{:S(2)}, u32[]{:S(2)}) async-start(s32[32,1,2]{2,1,0:T(1,128)} %bitcast), calls=%async_computation | async-start | bytes 32768 | tf_op jit(solution)/shard_map/all_to_all | solution.py:64
  34.7 2.3 constant_dynamic-update-slice_fusion.1
  38.1 8.4 %all-to-all-done = s32[32,1,2]{2,1,0:T(1,128)S(1)} async-done(((s32[32,1,2]{2,1,0:T(1,128)}), s32[32,1,2]{2,1,0:T(1,128)S(1)}, u32[]{:S(2)}, u32[]{:S(2)}) %all-to-all-start) | async-done | bytes 288 | tf_op jit(solution)/shard_map/all_to_all | solution.py:64
  47.8 29.4 %all-gather.2.cloned.1.call-done = bf16[16,64,2048]{2,1,0:T(8,128)(2,1)} async-done(((bf16[16,64,512]{2,1,0:T(8,128)(2,1)}), bf16[16,64,2048]{2,1,0:T(8,128)(2,1)}) %all-gather.2.cloned.1.call-update) | async-done | bytes 4194320 | tf_op jit(solution)/shard_map/all_gather | solution.py:66
  77.2 5.2 fusion.6
  84.8 3.6 copy.87
  88.4 13.3 %all-to-all-start.1 = ((bf16[32,2,64,512]{3,2,1,0:T(8,128)(2,1)}), bf16[32,2,64,512]{3,2,1,0:T(8,128)(2,1)}, u32[]{:S(2)}, u32[]{:S(2)}) async-start(bf16[32,2,64,512]{3,2,1,0:T(8,128)(2,1)} %bitcast.76), calls=%async_computation.1 | async-start | bytes 8388608 | tf_op jit(solution)/shard_map/all_to_all | solution.py:74
  101.8 183.2 %all-to-all-done.1 = bf16[32,2,64,512]{3,2,1,0:T(8,128)(2,1)} async-done(((bf16[32,2,64,512]{3,2,1,0:T(8,128)(2,1)}), bf16[32,2,64,512]{3,2,1,0:T(8,128)(2,1)}, u32[]{:S(2)}, u32[]{:S(2)}) %all-to-all-start.1) | async-done | bytes 4194336 | tf_op jit(solution)/shard_map/all_to_all | solution.py:74
  285.0 2.9 gather_fusion
  290.7 3.1 fusion.21
  293.8 2.9 fusion.10
  296.8 3.3 fusion.7
  300.0 1.8 multiply_reduce_fusion
  303.2 2.4 copy.77
  305.6 2.9 convert_element_type.78
  308.5 1.4 convolution_convert_fusion
  309.9 3.5 copy.88
  313.4 10.5 %all-to-all-start.3 = ((bf16[32,2,64,512]{3,2,1,0:T(8,128)(2,1)}), bf16[32,2,64,512]{3,2,1,0:T(8,128)(2,1)}, u32[]{:S(2)}, u32[]{:S(2)}) async-start(bf16[32,2,64,512]{3,2,1,0:T(8,128)(2,1)} %bitcast.77), calls=%async_computation.3 | async-start | bytes 8388608 | tf_op jit(solution)/shard_map/all_to_all | solution.py:135
  325.3 5.6 convolution_convert_fusion.4
  330.9 176.5 %all-to-all-done.3 = bf16[32,2,64,512]{3,2,1,0:T(8,128)(2,1)} async-done(((bf16[32,2,64,512]{3,2,1,0:T(8,128)(2,1)}), bf16[32,2,64,512]{3,2,1,0:T(8,128)(2,1)}, u32[]{:S(2)}, u32[]{:S(2)}) %all-to-all-start.3) | async-done | bytes 4194336 | tf_op jit(solution)/shard_map/all_to_all | solution.py:135
  507.4 6.0 all-to-all-start.2
  513.4 4.7 copy.89
  520.6 2.6 convolution_bitcast_fusion
  523.2 1.9 copy.78
  525.1 1.5 copy.79
  527.9 5.9 convolution_convert_fusion.3
  533.8 27.0 %all-to-all-done.2 = bf16[4,256,2048]{2,1,0:T(8,128)(2,1)} async-done(((bf16[4,256,2048]{2,1,0:T(8,128)(2,1)}), bf16[4,256,2048]{2,1,0:T(8,128)(2,1)}, u32[]{:S(2)}, u32[]{:S(2)}) %all-to-all-start.2) | async-done | bytes 4194336 | tf_op jit(solution)/shard_map/all_to_all | solution.py:37
  560.8 6.4 all-to-all-start.4
  567.9 4.3 reduce_sum.54
  572.2 41.5 %all-to-all-done.4 = bf16[4,4,64,2048]{3,2,1,0:T(8,128)(2,1)} async-done(((bf16[4,4,64,2048]{3,2,1,0:T(8,128)(2,1)}), bf16[4,4,64,2048]{3,2,1,0:T(8,128)(2,1)}, u32[]{:S(2)}, u32[]{:S(2)}) %all-to-all-start.4) | async-done | bytes 4194336 | tf_op jit(solution)/shard_map/all_to_all | solution.py:37
  613.7 4.3 reduce_sum.55
  617.9 21.3 %reduce-scatter.5.cloned.1.call-done = f32[1,64,256]{2,1,0:T(8,128)} async-done(((f32[16,64,256]{2,1,0:T(8,128)}), f32[1,64,256]{2,1,0:T(8,128)}) %reduce-scatter.5.cloned.1.call-update) | async-done | bytes 65552 | tf_op jit(solution)/shard_map/reduce_scatter | solution.py:21
  (64 shorter events, 17.6 us)
Async XLA Ops:
  7.2 280.7 %copy-start = (bf16[1024,256]{1,0:T(8,128)(2,1)S(1)}, bf16[1024,256]{1,0:T(8,128)(2,1)}, u32[]{:S(2)}) copy-start(bf16[1024,256]{1,0:T(8,128)(2,1)} %param.11) | copy-start | bytes 1572868
  7.2 29.8 %copy-start.6 = (bf16[2048,256]{1,0:T(8,128)(2,1)S(1)}, bf16[2048,256]{1,0:T(8,128)(2,1)}, u32[]{:S(2)}) copy-start(bf16[2048,256]{1,0:T(8,128)(2,1)} %param.16) | copy-start | bytes 3145732
  7.2 70.0 %all-gather.2.cloned.1.call-start = ((), (), s32[]{:S(2)}) async-start(), calls=%async_computation.7 | async-start | bytes 5242880 | tf_op jit(solution)/shard_map/all_gather | solution.py:66
  10.0 36.5 %all-to-all-start = ((s32[32,1,2]{2,1,0:T(1,128)}), s32[32,1,2]{2,1,0:T(1,128)S(1)}, u32[]{:S(2)}, u32[]{:S(2)}) async-start(s32[32,1,2]{2,1,0:T(1,128)} %bitcast), calls=%async_computation | async-start | bytes 32768 | tf_op jit(solution)/shard_map/all_to_all | solution.py:64
  88.4 196.6 %all-to-all-start.1 = ((bf16[32,2,64,512]{3,2,1,0:T(8,128)(2,1)}), bf16[32,2,64,512]{3,2,1,0:T(8,128)(2,1)}, u32[]{:S(2)}, u32[]{:S(2)}) async-start(bf16[32,2,64,512]{3,2,1,0:T(8,128)(2,1)} %bitcast.76), calls=%async_computation.1 | async-start | bytes 8388608 | tf_op jit(solution)/shard_map/all_to_all | solution.py:74
  287.9 12.1 %copy-start.2 = (bf16[32,64,512]{2,1,0:T(8,128)(2,1)}, bf16[32,64,512]{2,1,0:T(8,128)(2,1)S(1)}, u32[]{:S(2)}) copy-start(bf16[32,64,512]{2,1,0:T(8,128)(2,1)S(1)} %gather_fusion) | copy-start | bytes 6291460
  288.3 1.2 copy-start.5
  290.7 3.1 copy-start.10
  296.8 3.3 copy-start.12
  300.0 1.8 copy-start.4
  301.8 1.2 copy-start.9
  313.4 10.5 %copy-start.3 = (bf16[32,64,512]{2,1,0:T(8,128)(2,1)S(1)}, bf16[32,64,512]{2,1,0:T(8,128)(2,1)}, u32[]{:S(2)}) copy-start(bf16[32,64,512]{2,1,0:T(8,128)(2,1)} %copy-done.2) | copy-start | bytes 6291460
  313.4 194.0 %all-to-all-start.3 = ((bf16[32,2,64,512]{3,2,1,0:T(8,128)(2,1)}), bf16[32,2,64,512]{3,2,1,0:T(8,128)(2,1)}, u32[]{:S(2)}, u32[]{:S(2)}) async-start(bf16[32,2,64,512]{3,2,1,0:T(8,128)(2,1)} %bitcast.77), calls=%async_computation.3 | async-start | bytes 8388608 | tf_op jit(solution)/shard_map/all_to_all | solution.py:135
  323.9 1.0 copy-start.11
  323.9 1.4 copy-start.14
  507.4 53.4 %all-to-all-start.2 = ((bf16[4,256,2048]{2,1,0:T(8,128)(2,1)}), bf16[4,256,2048]{2,1,0:T(8,128)(2,1)}, u32[]{:S(2)}, u32[]{:S(2)}) async-start(bf16[4,256,2048]{2,1,0:T(8,128)(2,1)} %bitcast.87), calls=%async_computation.2 | async-start | bytes 8388608 | tf_op jit(solution)/shard_map/all_to_all | solution.py:37
  513.4 53.7 %reduce-scatter.3.cloned.1.call-start = ((), (), s32[]{:S(2)}) async-start(), calls=%async_computation.8 | async-start | bytes 3145728 | tf_op jit(solution)/shard_map/reduce_scatter | solution.py:21
  518.1 2.5 copy-start.13
  519.2 1.0 copy-start.7
  526.7 1.2 copy-start.8
  560.8 52.9 %all-to-all-start.4 = ((bf16[4,4,64,2048]{3,2,1,0:T(8,128)(2,1)}), bf16[4,4,64,2048]{3,2,1,0:T(8,128)(2,1)}, u32[]{:S(2)}, u32[]{:S(2)}) async-start(bf16[4,4,64,2048]{3,2,1,0:T(8,128)(2,1)} %bitcast.88), calls=%async_computation.4 | async-start | bytes 8388608 | tf_op jit(solution)/shard_map/all_to_all | solution.py:37
  567.1 72.1 %reduce-scatter.5.cloned.1.call-start = ((), (), s32[]{:S(2)}) async-start(), calls=%async_computation.9 | async-start | bytes 1114112 | tf_op jit(solution)/shard_map/reduce_scatter | solution.py:21
  567.9 71.3 %copy-start.1 = (bf16[1024,256]{1,0:T(8,128)(2,1)S(1)}, bf16[1024,256]{1,0:T(8,128)(2,1)}, u32[]{:S(2)}) copy-start(bf16[1024,256]{1,0:T(8,128)(2,1)} %param.11) | copy-start | bytes 1572868
Sparse Core Ops, SparseCore 0:
  9.9 67.3 all-gather.1
  526.9 17.2 reduce-scatter.2
  571.0 68.1 reduce-scatter.4
where the time goes:
time: 647 us; the launch traced here: 646 us
  waiting for transfers between devices  489 us (76%)
  starting transfers between devices  61 us (9%)
  local copies, waits for them, and re-layouts  35.7 us (6%)
  matrix products  32.1 us (5%)
  other arithmetic  14.1 us (2%)
  between operations  14.1 us (2%)
    all_to_all x1, waiting for transfers between devices, local(): lax.all_to_all(outgoing.reshape(st_count, slot_depth, pass_len, pair_cols...  183 us
    all_to_all x1, waiting for transfers between devices, local(): lax.all_to_all(returning.reshape(st_count, slot_depth, pass_len, pair_col...  176 us
    all_to_all x2, waiting for transfers between devices, summed_on_arrival(): lax.all_to_all(in_blocks(array, dim, devices), axis, 0, 0, tiled=True)  68.5 us
    all_gather x1, waiting for transfers between devices, local(): gathered = lax.all_gather(store, 'tp', axis=2, tiled=True)  29.4 us
    all_to_all x1, starting transfers between devices, local(): lax.all_to_all(wanted, ST, split_axis=0, concat_axis=0, tiled=True)  24.7 us
    reduce_scatter x2, waiting for transfers between devices, sum_in_order(): tiles = lax.psum_scatter(tiles, axes[k], scatter_dimension=0, tiled=True)  21.3 us
    unnamed x36, local copies, waits for them, and re-layouts  20.5 us
    all_to_all x1, starting transfers between devices, local(): lax.all_to_all(outgoing.reshape(st_count, slot_depth, pass_len, pair_cols...  13.3 us
  transfers between devices with their start and end apart: 8, of which 7 were waited for; matrix products, arithmetic and copies ran while one was open for 6% of the time, Pallas kernels for 0%

commit v1 on v0

--- a/solution.py
+++ b/solution.py
@@ -63,7 +63,9 @@
     wanted = jnp.max(jnp.where(slot_hot, within[:, None], -1), axis=0).reshape(st_count, slot_depth)
     asked_rows = lax.all_to_all(wanted, ST, split_axis=0, concat_axis=0, tiled=True).reshape(-1)
     weight_kv = jnp.concatenate([w_key, w_value], axis=1)
-    gathered = lax.all_gather(store, "tp", axis=2, tiled=True)
+    gathered = jnp.concatenate(
+        lax.all_to_all(jnp.stack([store] * lax.axis_size("tp")), "tp", 0, 0), axis=2
+    )
     flat_rows = gathered.reshape(passages * pass_len, model_width)
     kv_pass = jnp.dot(flat_rows, weight_kv, preferred_element_type=jnp.float32)
     kv_low = kv_pass.astype(jnp.bfloat16).reshape(passages, pass_len * pair_cols)

time: 647 us -> 675 us (1.043)
  blocking collectives: 0 us -> 36.4 us
  starting transfers between devices: 61 us -> 29.4 us
  waiting for transfers between devices: 489 us -> 502 us
  local copies, waits for them, and re-layouts: 35.7 us -> 47.3 us
    all_to_all x0 -> x1, blocking collectives: none -> 36.4 us  [local(): lax.all_to_all(wanted, ST, split_axis=0, concat_axis=0, tiled=True)]
    all_to_all x1, waiting for transfers between devices: 8.36 us -> 43.7 us  [local(): lax.all_to_all(jnp.stack([store] * lax.axis_size('tp')), 'tp', 0, 0)]
    all_gather x1 -> x0, waiting for transfers between devices: 29.4 us -> none  [local(): gathered = lax.all_gather(store, 'tp', axis=2, tiled=True)]
    all_to_all x1, starting transfers between devices: 24.7 us -> 5.36 us  [local(): lax.all_to_all(jnp.stack([store] * lax.axis_size('tp')), 'tp', 0, 0)]
    all_to_all x2, waiting for transfers between devices: 68.5 us -> 56 us  [summed_on_arrival(): lax.all_to_all(in_blocks(array, dim, devices), axis, 0, 0, tiled=True)]
    all_to_all x1, starting transfers between devices: 13.3 us -> 5.84 us  [local(): lax.all_to_all(outgoing.reshape(st_count, slot_depth, pass_len, pair_cols...]
    all_to_all x1, waiting for transfers between devices: 176 us -> 184 us  [local(): lax.all_to_all(returning.reshape(st_count, slot_depth, pass_len, pair_col...]
    all_to_all x1, waiting for transfers between devices: 183 us -> 190 us  [local(): lax.all_to_all(outgoing.reshape(st_count, slot_depth, pass_len, pair_cols...]
  transfers between devices with their start and end apart: 8 -> 7, of which waited for: 7 -> 6; matrix products, arithmetic and copies ran while one was open for 6% -> 5% of each run, Pallas kernels for 0% -> 0%
where the time goes in v1:
time: 675 us; the launch traced here: 674 us
  waiting for transfers between devices  502 us (74%)
  local copies, waits for them, and re-layouts  47.3 us (7%)
  blocking collectives  36.4 us (5%)
  matrix products  30.9 us (5%)
  starting transfers between devices  29.4 us (4%)
  between operations  14.4 us (2%)
  other arithmetic  14.1 us (2%)
    all_to_all x1, waiting for transfers between devices, local(): lax.all_to_all(outgoing.reshape(st_count, slot_depth, pass_len, pair_cols...  190 us
    all_to_all x1, waiting for transfers between devices, local(): lax.all_to_all(returning.reshape(st_count, slot_depth, pass_len, pair_col...  184 us
    all_to_all x2, waiting for transfers between devices, summed_on_arrival(): lax.all_to_all(in_blocks(array, dim, devices), axis, 0, 0, tiled=True)  56 us
    all_to_all x1, waiting for transfers between devices, local(): lax.all_to_all(jnp.stack([store] * lax.axis_size('tp')), 'tp', 0, 0)  43.7 us
    all_to_all x1, blocking collectives, local(): lax.all_to_all(wanted, ST, split_axis=0, concat_axis=0, tiled=True)  36.4 us
    reduce_scatter x2, waiting for transfers between devices, sum_in_order(): tiles = lax.psum_scatter(tiles, axes[k], scatter_dimension=0, tiled=True)  27.2 us
    unnamed x41, local copies, waits for them, and re-layouts  23.1 us
  transfers between devices with their start and end apart: 7, of which 6 were waited for; matrix products, arithmetic and copies ran while one was open for 5% of the time, Pallas kernels for 0%

profile of v1, /device:TPU:34, one launch (start us, length us, event | category | flops | bytes accessed | tf_op | source)
XLA Modules:
  0.0 674.2 jit_solution(18394513524802144891)
XLA Ops:
  8.6 36.4 %all_to_all.34 = s32[32,1,2]{2,1,0:T(1,128)S(1)} all-to-all(s32[32,1,2]{2,1,0:T(1,128)S(1)} %bitcast.102), channel_id=1, replica_groups=mesh['grp'=2,'st_0'=16,'st_1'=2,'tp'=4] {'st_0','st_1'}, dimensions={0} | all-to-all | bytes 512 | tf_op jit(solution)/shard_map/all_to_all | solution.py:64
  45.0 3.8 stack.2
  48.7 5.4 all-to-all-start.1
  58.1 43.7 %all-to-all-done.1 = bf16[4,16,64,512]{3,2,1,0:T(8,128)(2,1)} async-done(((bf16[4,16,64,512]{3,2,1,0:T(8,128)(2,1)}), bf16[4,16,64,512]{3,2,1,0:T(8,128)(2,1)}, u32[]{:S(2)}, u32[]{:S(2)}) %all-to-all-start.1) | async-done | bytes 4194336 | tf_op jit(solution)/shard_map/all_to_all | solution.py:67
  101.8 5.7 copy.68
  109.0 1.9 copy-done.4
  110.9 4.0 fusion.6
  117.2 3.6 copy.90
  120.8 5.8 all-to-all-start.2
  126.7 190.3 %all-to-all-done.2 = bf16[32,2,64,512]{3,2,1,0:T(8,128)(2,1)} async-done(((bf16[32,2,64,512]{3,2,1,0:T(8,128)(2,1)}), bf16[32,2,64,512]{3,2,1,0:T(8,128)(2,1)}, u32[]{:S(2)}, u32[]{:S(2)}) %all-to-all-start.2) | async-done | bytes 4194336 | tf_op jit(solution)/shard_map/all_to_all | solution.py:76
  317.1 2.9 gather_fusion
  322.8 3.1 fusion.21
  325.9 2.9 fusion.10
  328.8 3.3 fusion.7
  332.1 1.8 multiply_reduce_fusion
  335.3 2.4 copy.79
  337.7 2.9 convert_element_type.78
  341.9 3.5 copy.91
  345.5 5.8 all-to-all-start.4
  352.7 5.6 convolution_convert_fusion.4
  358.3 183.7 %all-to-all-done.4 = bf16[32,2,64,512]{3,2,1,0:T(8,128)(2,1)} async-done(((bf16[32,2,64,512]{3,2,1,0:T(8,128)(2,1)}), bf16[32,2,64,512]{3,2,1,0:T(8,128)(2,1)}, u32[]{:S(2)}, u32[]{:S(2)}) %all-to-all-start.4) | async-done | bytes 4194336 | tf_op jit(solution)/shard_map/all_to_all | solution.py:137
  541.9 6.1 all-to-all-start.3
  548.0 4.7 copy.92
  555.2 2.6 convolution_bitcast_fusion
  557.8 1.9 copy.80
  562.5 5.9 convolution_convert_fusion.3
  568.4 20.8 %all-to-all-done.3 = bf16[4,256,2048]{2,1,0:T(8,128)(2,1)} async-done(((bf16[4,256,2048]{2,1,0:T(8,128)(2,1)}), bf16[4,256,2048]{2,1,0:T(8,128)(2,1)}, u32[]{:S(2)}, u32[]{:S(2)}) %all-to-all-start.3) | async-done | bytes 4194336 | tf_op jit(solution)/shard_map/all_to_all | solution.py:37
  589.2 6.4 all-to-all-start.5
  596.3 4.3 reduce_sum.54
  600.6 35.2 %all-to-all-done.5 = bf16[4,4,64,2048]{3,2,1,0:T(8,128)(2,1)} async-done(((bf16[4,4,64,2048]{3,2,1,0:T(8,128)(2,1)}), bf16[4,4,64,2048]{3,2,1,0:T(8,128)(2,1)}, u32[]{:S(2)}, u32[]{:S(2)}) %all-to-all-start.5) | async-done | bytes 4194336 | tf_op jit(solution)/shard_map/all_to_all | solution.py:37
  635.8 4.3 reduce_sum.55
  640.1 27.2 %reduce-scatter.5.cloned.1.call-done = f32[1,64,256]{2,1,0:T(8,128)} async-done(((f32[16,64,256]{2,1,0:T(8,128)}), f32[1,64,256]{2,1,0:T(8,128)}) %reduce-scatter.5.cloned.1.call-update) | async-done | bytes 65552 | tf_op jit(solution)/shard_map/reduce_scatter | solution.py:21
  (70 shorter events, 22.2 us)
Async XLA Ops:
  7.2 312.8 %copy-start = (bf16[1024,256]{1,0:T(8,128)(2,1)S(1)}, bf16[1024,256]{1,0:T(8,128)(2,1)}, u32[]{:S(2)}) copy-start(bf16[1024,256]{1,0:T(8,128)(2,1)} %param.11) | copy-start | bytes 1572868
  48.7 5.4 copy-start.10
  48.7 53.1 %all-to-all-start.1 = ((bf16[4,16,64,512]{3,2,1,0:T(8,128)(2,1)}), bf16[4,16,64,512]{3,2,1,0:T(8,128)(2,1)}, u32[]{:S(2)}, u32[]{:S(2)}) async-start(bf16[4,16,64,512]{3,2,1,0:T(8,128)(2,1)} %stack.2), calls=%async_computation.1 | async-start | bytes 8388608 | tf_op jit(solution)/shard_map/all_to_all | solution.py:67
  54.1 1.6 copy-start.11
  108.9 1.9 copy-start.4
  120.8 196.3 %all-to-all-start.2 = ((bf16[32,2,64,512]{3,2,1,0:T(8,128)(2,1)}), bf16[32,2,64,512]{3,2,1,0:T(8,128)(2,1)}, u32[]{:S(2)}, u32[]{:S(2)}) async-start(bf16[32,2,64,512]{3,2,1,0:T(8,128)(2,1)} %bitcast.79), calls=%async_computation.2 | async-start | bytes 8388608 | tf_op jit(solution)/shard_map/all_to_all | solution.py:76
  320.0 12.2 %copy-start.2 = (bf16[32,64,512]{2,1,0:T(8,128)(2,1)}, bf16[32,64,512]{2,1,0:T(8,128)(2,1)S(1)}, u32[]{:S(2)}) copy-start(bf16[32,64,512]{2,1,0:T(8,128)(2,1)S(1)} %gather_fusion) | copy-start | bytes 6291460
  320.4 1.2 copy-start.7
  322.8 3.1 copy-start.13
  328.8 3.3 copy-start.15
  332.1 1.8 copy-start.6
  333.9 1.2 copy-start.12
  345.5 5.8 copy-start.3
  345.5 196.4 %all-to-all-start.4 = ((bf16[32,2,64,512]{3,2,1,0:T(8,128)(2,1)}), bf16[32,2,64,512]{3,2,1,0:T(8,128)(2,1)}, u32[]{:S(2)}, u32[]{:S(2)}) async-start(bf16[32,2,64,512]{3,2,1,0:T(8,128)(2,1)} %bitcast.80), calls=%async_computation.4 | async-start | bytes 8388608 | tf_op jit(solution)/shard_map/all_to_all | solution.py:137
  351.3 1.0 copy-start.14
  351.3 1.4 copy-start.16
  541.9 47.3 %all-to-all-start.3 = ((bf16[4,256,2048]{2,1,0:T(8,128)(2,1)}), bf16[4,256,2048]{2,1,0:T(8,128)(2,1)}, u32[]{:S(2)}, u32[]{:S(2)}) async-start(bf16[4,256,2048]{2,1,0:T(8,128)(2,1)} %bitcast.93), calls=%async_computation.3 | async-start | bytes 8388608 | tf_op jit(solution)/shard_map/all_to_all | solution.py:37
  548.0 47.5 %reduce-scatter.3.cloned.1.call-start = ((), (), s32[]{:S(2)}) async-start(), calls=%async_computation.8 | async-start | bytes 3145728 | tf_op jit(solution)/shard_map/reduce_scatter | solution.py:21
  552.7 2.5 copy-start.5
  553.9 1.0 copy-start.8
  561.3 1.2 copy-start.9
  589.2 46.7 %all-to-all-start.5 = ((bf16[4,4,64,2048]{3,2,1,0:T(8,128)(2,1)}), bf16[4,4,64,2048]{3,2,1,0:T(8,128)(2,1)}, u32[]{:S(2)}, u32[]{:S(2)}) async-start(bf16[4,4,64,2048]{3,2,1,0:T(8,128)(2,1)} %bitcast.94), calls=%async_computation.5 | async-start | bytes 8388608 | tf_op jit(solution)/shard_map/all_to_all | solution.py:37
  595.5 71.8 %reduce-scatter.5.cloned.1.call-start = ((), (), s32[]{:S(2)}) async-start(), calls=%async_computation.9 | async-start | bytes 1114112 | tf_op jit(solution)/shard_map/reduce_scatter | solution.py:21
  596.3 71.0 %copy-start.1 = (bf16[1024,256]{1,0:T(8,128)(2,1)S(1)}, bf16[1024,256]{1,0:T(8,128)(2,1)}, u32[]{:S(2)}) copy-start(bf16[1024,256]{1,0:T(8,128)(2,1)} %param.11) | copy-start | bytes 1572868
Sparse Core Ops, SparseCore 0:
  561.5 10.7 reduce-scatter.2
  599.4 67.8 reduce-scatter.4
